TPU v7x, 32 devices: a whole 2x2x4 slice. The times are simulated.
32 devices in a mesh: sp: 8 (over z, y), tp: 4 (over x, core).
Axes of the slice: x: 2, y: 2, z: 4, core: 2. Of those that a mesh axis runs over, the one named last changes fastest.
Arguments:
- stream: bfloat16 [2048, 2048], P('sp', 'tp'), may hold values from -8 to 8
- norm_gain: float32 [2, 2048], P(None, 'tp'), may hold values from 0.1 to 1.9
- query_weight: bfloat16 [2, 2048, 1024], P(None, None, 'tp'), may hold values from -4 to 4
- key_weight: bfloat16 [2, 2048, 1024], P(None, None, 'tp'), may hold values from -4 to 4
- value_weight: bfloat16 [2, 2048, 1024], P(None, None, 'tp'), may hold values from -0.125 to 0.125
- out_weight: bfloat16 [2, 1024, 2048], P(None, None, 'tp'), may hold values from -1.5 to 1.5
- rel_bias: float32 [2, 16, 257], P(None, 'tp'), may hold values from -4 to 4
Outputs:
- mixed: bfloat16 [2048, 2048], P('sp', 'tp')
All inputs are finite; a program needn't handle non-finite values.
Results may differ from a plain program's by a relative error of at most 0.013.
Values may be sent and summed in bfloat16 or wider, within the bound.
A program may use at most 64 MiB of HBM per device.

v0:
```python
import functools

import jax
import jax.numpy as jnp
from jax import lax
from jax.experimental import pallas as pl
from jax.experimental.pallas import tpu as pltpu
from jax.sharding import PartitionSpec as P

SEG = 64
PREV = 8
CLIP = 128
LANES = 128
CHUNKS = 4
PAIR = 2 * SEG
REACH = PREV * SEG
BAND = REACH + PAIR

epsilon = 1e-06
masked_score = -1e30
MESH = pl.DeviceIdType.MESH


class Gather:
    def __init__(self, n_tp, slot, send_sems, recv_sems):
        self.n_x = n_tp // 2
        self.me = lax.axis_index("tp")
        self.core = lax.rem(self.me, 2)
        self.x = self.me // 2
        self.sibling = self.me + 1 - 2 * self.core
        self.slot, self.send_sems, self.recv_sems = slot, send_sems, recv_sems

    def across(self, step, core):
        return lax.rem(self.x + step, self.n_x) * 2 + core

    def copy(self, source, origin, part, index, target):
        return pltpu.make_async_remote_copy(
            src_ref=source,
            dst_ref=self.slot(origin, part),
            send_sem=self.send_sems.at[part, index],
            recv_sem=self.recv_sems.at[part, origin],
            device_id={"tp": target},
            device_id_type=MESH,
        )

    def own(self, part, source=None):
        source = self.slot(self.me, part) if source is None else source
        targets = [self.across(s, self.core) for s in range(1, self.n_x)] + [self.sibling]
        return [self.copy(source, self.me, part, i, t) for i, t in enumerate(targets)]

    def send(self, part, source=None):
        for copy in self.own(part, source):
            copy.start()

    def relays(self, part):
        out = []
        for s in range(1, self.n_x):
            origin = self.across(s, self.core)
            out.append(
                self.copy(self.slot(origin, part), origin, part, self.n_x - 1 + s, self.sibling)
            )
        return out

    def relay(self, part):
        for copy in self.relays(part):
            copy.wait_recv()
            copy.start()

    def others(self):
        return [self.sibling] + [self.across(s, 1 - self.core) for s in range(1, self.n_x)]

    def wait_slot(self, part, origin):
        self.copy(self.slot(origin, part), origin, part, 0, self.sibling).wait_recv()

    def wait_rest(self, part):
        for origin in self.others():
            self.wait_slot(part, origin)

    def finish(self, part, source=None):
        for copy in self.own(part, source) + self.relays(part):
            copy.wait_send()


def kernel(
    n_tp, n_sp, head_dim,
    stream, gain, query_w, key_w, value_w, out_w, rel_bias,
    out,
    xg, gg, table, wq, wk, wv, wo, normed, bias, qx, kx, vx, att,
    xs, xr, ats, atr, kvs, kvr, gs, gr, wsem, own_sem,
):
    layers, _, rows, width = xg.shape
    groups = kx.shape[1]
    head_cols = groups * LANES
    per_group = LANES // head_dim
    total_width = n_tp * width
    shift = REACH // rows
    sp = lax.axis_index("sp")
    tp = lax.axis_index("tp")
    relayed = shift == 2 and n_sp % 2 == 0
    blocks = rows // PAIR
    per_block = CHUNKS // blocks

    weights = []
    for l in range(layers):
        pairs = ((key_w, wk), (value_w, wv), (query_w, wq), (out_w, wo))
        weights.append(
            [pltpu.make_async_copy(s.at[l], d.at[l], wsem.at[l, i]) for i, (s, d) in enumerate(pairs)]
        )
    own_stream = pltpu.make_async_copy(stream, xg.at[0, tp], own_sem.at[0])
    own_gain = pltpu.make_async_copy(gain, gg.at[tp], own_sem.at[1])
    own_stream.start()
    own_gain.start()
    own_table = pltpu.make_async_copy(rel_bias, table, own_sem.at[2])
    own_table.start()

    barrier = pltpu.get_barrier_semaphore()
    for d in range(1, n_tp):
        pl.semaphore_signal(
            barrier, inc=1, device_id={"tp": lax.rem(tp + d, n_tp)}, device_id_type=MESH
        )
    count = n_tp - 1
    for d in range(1, shift + 1):

        @pl.when(sp + d < n_sp)
        def _():
            pl.semaphore_signal(barrier, inc=1, device_id={"sp": sp + d}, device_id_type=MESH)

        @pl.when(sp >= d)
        def _():
            pl.semaphore_signal(barrier, inc=1, device_id={"sp": sp - d}, device_id_type=MESH)

        count = count + jnp.where(sp + d < n_sp, 1, 0) + jnp.where(sp >= d, 1, 0)
    for copy in weights[0]:
        copy.start()
    pl.semaphore_wait(barrier, count)

    piece = rows // CHUNKS
    xgather = [
        Gather(
            n_tp,
            lambda j, c, l=l: xg.at[l, j, pl.ds(c * piece, piece)],
            xs.at[l],
            xr.at[l],
        )
        for l in range(layers)
    ]
    agather = [
        Gather(n_tp, lambda j, b, l=l: att.at[l, j, b], ats.at[l], atr.at[l])
        for l in range(layers)
    ]

    own_stream.wait()
    for c in range(CHUNKS):
        xgather[0].send(c)
    gain_copies = [
        pltpu.make_async_remote_copy(
            src_ref=gain,
            dst_ref=gg.at[tp],
            send_sem=gs.at[d - 1],
            recv_sem=gr.at[d - 1],
            device_id={"tp": lax.rem(tp + d, n_tp)},
            device_id_type=MESH,
        )
        for d in range(1, n_tp)
    ]
    for copy in gain_copies:
        copy.start()
    for l in range(1, layers):
        for copy in weights[l]:
            copy.start()

    for l in range(layers):
        for d in range(1, shift + 1):

            @pl.when(sp < d)
            def _():
                empty = jnp.zeros((rows, LANES), jnp.bfloat16)
                for g in range(groups):
                    kx[l, g, pl.ds((shift - d) * rows, rows), :] = empty
                    vx[l, g, pl.ds((shift - d) * rows, rows), :] = empty

    own_table.wait()
    near = 2 * CLIP
    flip = (
        lax.broadcasted_iota(jnp.int32, (near, near), 0)
        + lax.broadcasted_iota(jnp.int32, (near, near), 1)
        == near - 1
    ).astype(jnp.float32)
    seg_q = lax.broadcasted_iota(jnp.int32, (PAIR, BAND), 0) // SEG
    seg_k = lax.broadcasted_iota(jnp.int32, (PAIR, BAND), 1) // SEG
    seen = (seg_k >= seg_q) & (seg_k <= seg_q + PREV)
    for l in range(layers):
        heads = table.shape[1]
        turned = jnp.dot(
            table[l][:, 1:], flip, precision=lax.Precision.HIGHEST,
            preferred_element_type=jnp.float32,
        )
        far = table[l][:, near:]
        base = jnp.concatenate(
            [
                jnp.broadcast_to(far, (heads, REACH - CLIP)),
                turned,
                jnp.broadcast_to(far, (heads, PAIR)),
            ],
            axis=1,
        )
        for h in range(heads):
            spread = jnp.broadcast_to(base[h : h + 1], (PAIR, base.shape[1]))
            shifted = pltpu.roll(spread, 0, 1, stride=1, stride_axis=0)[:, :BAND]
            first = h % per_group * PAIR
            bias[l, h // per_group, first : first + PAIR, :] = jnp.where(
                seen, shifted, masked_score
            )

    tensors = (kx, vx)

    def halo_copy(l, t, g, half, from_slot, to_slot, index, target):
        buf = tensors[t]
        return pltpu.make_async_remote_copy(
            src_ref=buf.at[l, g, pl.ds(from_slot * rows + half * PAIR, PAIR)],
            dst_ref=buf.at[l, g, pl.ds(to_slot * rows + half * PAIR, PAIR)],
            send_sem=kvs.at[l, t, g * blocks + half, index],
            recv_sem=kvr.at[l, t, g * blocks + half, to_slot],
            device_id={"sp": target},
            device_id_type=MESH,
        )

    even = lax.rem(sp, 2) == 0
    odd_behind = (lax.rem(sp, 2) == 1) & (sp >= 2)

    def direct_copies(l, t, g, half):
        out_list = []
        for d in range(shift, 0, -1):
            ok = sp + d < n_sp
            if relayed and d == 1:
                ok = even
            out_list.append((ok, halo_copy(l, t, g, half, shift, shift - d, d - 1, sp + d)))
        return out_list

    def relay_copy(l, t, g, half):
        return halo_copy(l, t, g, half, 0, 1, shift, sp - 1)

    def halo_send(l, t, half):
        for g in range(groups):
            for ok, copy in direct_copies(l, t, g, half):
                pl.when(ok)(copy.start)

    def halo_wait_slot(l, t, g, half, d):
        @pl.when(sp >= d)
        def _():
            slot = shift - d
            halo_copy(l, t, g, half, slot, slot, 0, lax.rem(sp + 1, n_sp)).wait_recv()

    def halo_far(l, half):
        for t in range(2):
            for g in range(groups):
                halo_wait_slot(l, t, g, half, shift)
                if relayed:
                    pl.when(odd_behind)(relay_copy(l, t, g, half).start)

    def halo_near(l, g, half):
        for t in range(2):
            for d in range(shift - 1, 0, -1):
                halo_wait_slot(l, t, g, half, d)

    own_gain.wait()
    for d in range(1, n_tp):
        pltpu.make_async_remote_copy(
            src_ref=gain,
            dst_ref=gg.at[lax.rem(tp - d + n_tp, n_tp)],
            send_sem=gs.at[d - 1],
            recv_sem=gr.at[d - 1],
            device_id={"tp": lax.rem(tp + d, n_tp)},
            device_id_type=MESH,
        ).wait_recv()

    lane = lax.broadcasted_iota(jnp.int32, (PAIR, LANES), 1) // head_dim
    scale = head_dim ** (-0.5)

    def normalize(l, c):
        span = slice(c * piece, (c + 1) * piece)
        squares = jnp.zeros((piece, 1), jnp.float32)
        for j in range(n_tp):
            part = xg[l, j, span, :].astype(jnp.float32)
            squares = squares + jnp.sum(part * part, axis=-1, keepdims=True)
        inverse = lax.rsqrt(squares / total_width + epsilon)
        for j in range(n_tp):
            part = xg[l, j, span, :].astype(jnp.float32) * inverse
            normed[span, j * width : (j + 1) * width] = (
                part * gg[j, l : l + 1, :]
            ).astype(jnp.bfloat16)

    def block_rows(b):
        return slice(b * PAIR, (b + 1) * PAIR)

    def keys_values(l, b):
        for t, (buf, mat) in enumerate(((kx, wk), (vx, wv))):
            if b == 0:
                weights[l][t].wait()
            made = jnp.dot(normed[block_rows(b), :], mat[l], preferred_element_type=jnp.float32)
            made = made.astype(jnp.bfloat16)
            first = shift * rows + b * PAIR
            for g in range(groups):
                buf[l, g, first : first + PAIR, :] = made[:, g * LANES : (g + 1) * LANES]
            halo_send(l, t, b)

    def attend(l, b, g):
        lanes = slice(g * LANES, (g + 1) * LANES)
        block = qx[block_rows(b), lanes]
        stacked = jnp.concatenate(
            [jnp.where(lane == h, block, jnp.zeros_like(block)) for h in range(per_group)], axis=0
        )
        keys = kx[l, g, b * PAIR : b * PAIR + BAND, :]
        values = vx[l, g, b * PAIR : b * PAIR + BAND, :]
        position = sp * rows - REACH + b * PAIR + lax.broadcasted_iota(jnp.int32, (1, BAND), 1)
        hidden = jnp.where(position >= 0, 0.0, masked_score)
        scores = lax.dot_general(
            stacked, keys, (((1,), (1,)), ((), ())), preferred_element_type=jnp.float32
        )
        scores = scores + bias[l, g] + hidden
        top = jnp.max(scores, axis=-1, keepdims=True)
        grown = jnp.exp(scores - top)
        summed = jnp.sum(grown, axis=-1, keepdims=True)
        mix = jnp.dot(grown.astype(jnp.bfloat16), values, preferred_element_type=jnp.float32)
        mix = mix / summed
        chosen = mix[:PAIR]
        for h in range(1, per_group):
            chosen = jnp.where(lane == h, mix[h * PAIR : (h + 1) * PAIR], chosen)
        att[l, tp, b, :, lanes] = chosen.astype(jnp.bfloat16)

    def mixed_part(l, b, j):
        mat = wo[l, pl.ds(pl.multiple_of(j * head_cols, LANES), head_cols), :]
        return jnp.dot(att[l, j, b], mat, preferred_element_type=jnp.float32)

    for l in range(layers):
        gather = xgather[l]
        gather.relay(0)
        for b in range(blocks):
            for c in range(b * per_block, (b + 1) * per_block):
                if c + 1 < CHUNKS:
                    gather.relay(c + 1)
                gather.wait_rest(c)
                normalize(l, c)
            keys_values(l, b)
        weights[l][2].wait()
        for b in range(blocks):
            if b + 1 < blocks:
                halo_far(l, b)
            qx[block_rows(b), :] = (
                jnp.dot(normed[block_rows(b), :], wq[l], preferred_element_type=jnp.float32) * scale
            ).astype(jnp.bfloat16)
        halo_far(l, blocks - 1)
        for b in range(blocks):
            for g in range(groups):
                if b == 0:
                    for half in range(blocks):
                        halo_near(l, g, half)
                attend(l, b, g)
            agather[l].send(b)

        gather = agather[l]
        weights[l][3].wait()
        gather.relay(0)
        for b in range(blocks):
            total = xg[l, tp, block_rows(b), :].astype(jnp.float32) + mixed_part(l, b, tp)
            for s in range(1, gather.n_x):
                total = total + mixed_part(l, b, gather.across(s, gather.core))
            if b + 1 < blocks:
                gather.relay(b + 1)
            for origin in gather.others():
                gather.wait_slot(b, origin)
                total = total + mixed_part(l, b, origin)
            result = total.astype(jnp.bfloat16)
            if l + 1 < layers:
                xg[l + 1, tp, block_rows(b), :] = result
                for c in range(b * per_block, (b + 1) * per_block):
                    xgather[l + 1].send(c)
            else:
                out[block_rows(b), :] = result

    for copy in gain_copies:
        copy.wait_send()
    for l in range(layers):
        for c in range(CHUNKS):
            xgather[l].finish(c)
        for b in range(blocks):
            agather[l].finish(b)
            for g in range(groups):
                for t in range(2):
                    for ok, copy in direct_copies(l, t, g, b):
                        pl.when(ok)(copy.wait_send)
                    if relayed:
                        pl.when(odd_behind)(relay_copy(l, t, g, b).wait_send)


def per_device(n_tp, n_sp, stream, norm_gain, query_weight, key_weight, value_weight, out_weight, rel_bias):
    rows, width = stream.shape
    layers, full, head_cols = query_weight.shape
    heads_here = rel_bias.shape[1]
    head_dim = head_cols // heads_here
    groups = head_cols // LANES
    n_x = n_tp // 2
    shift = REACH // rows
    blocks = rows // PAIR
    any_space = pl.BlockSpec(memory_space=pltpu.HBM)
    vmem = pl.BlockSpec(memory_space=pltpu.VMEM)
    bf16, f32 = jnp.bfloat16, jnp.float32
    dma = pltpu.SemaphoreType.DMA
    return pl.pallas_call(
        functools.partial(kernel, n_tp, n_sp, head_dim),
        out_shape=jax.ShapeDtypeStruct((rows, width), bf16),
        in_specs=[any_space] * 7,
        out_specs=vmem,
        scratch_shapes=[
            pltpu.VMEM((layers, n_tp, rows, width), bf16),
            pltpu.VMEM((n_tp, layers, width), f32),
            pltpu.VMEM(rel_bias.shape, f32),
            pltpu.VMEM((layers, full, head_cols), bf16),
            pltpu.VMEM((layers, full, head_cols), bf16),
            pltpu.VMEM((layers, full, head_cols), bf16),
            pltpu.VMEM((layers, n_tp * head_cols, width), bf16),
            pltpu.VMEM((rows, full), bf16),
            pltpu.VMEM((layers, groups, (LANES // head_dim) * PAIR, BAND), f32),
            pltpu.VMEM((rows, head_cols), bf16),
            pltpu.VMEM((layers, groups, REACH + rows, LANES), bf16),
            pltpu.VMEM((layers, groups, REACH + rows, LANES), bf16),
            pltpu.VMEM((layers, n_tp, blocks, PAIR, head_cols), bf16),
            dma((layers, CHUNKS, 2 * n_x - 1)),
            dma((layers, CHUNKS, n_tp)),
            dma((layers, blocks, 2 * n_x - 1)),
            dma((layers, blocks, n_tp)),
            dma((layers, 2, groups * blocks, shift + 1)),
            dma((layers, 2, groups * blocks, shift)),
            dma((n_tp - 1,)),
            dma((n_tp - 1,)),
            dma((layers, 4)),
            dma((3,)),
        ],
        compiler_params=pltpu.CompilerParams(
            collective_id=0, has_side_effects=True, vmem_limit_bytes=60 * 1024 * 1024
        ),
    )(stream, norm_gain, query_weight, key_weight, value_weight, out_weight, rel_bias)


def solution(mesh):
    placed = (
        P("sp", "tp"),
        P(None, "tp"),
        P(None, None, "tp"),
        P(None, None, "tp"),
        P(None, None, "tp"),
        P(None, None, "tp"),
        P(None, "tp", None),
    )
    return jax.shard_map(
        functools.partial(per_device, mesh.shape["tp"], mesh.shape["sp"]),
        mesh=mesh, in_specs=placed, out_specs=P("sp", "tp"), check_vma=False,
    )
```

profile of v0, /device:TPU:17, one launch (start us, length us, event | category | flops | bytes accessed | tf_op | source)
XLA Modules:
  0.0 53.1 jit_solution(15203858230997599232)
XLA Ops:
  0.0 51.4 %shard_map.73 = bf16[256,512]{1,0:T(8,128)(2,1)} custom-call(bf16[256,512]{1,0:T(8,128)(2,1)} %stream.1, f32[2,512]{1,0:T(2,128)} %gain.1, bf16[2,2048,256]{2,1,0:T(8,128)(2,1)} %query_w.1, bf16[2,2048,256]{2,1,0:T(8,128)(2,1)} %key_w.1, bf16[2,2048,256]{2,1,0:T(8,128)(2,1)} %value_w.1, bf16[2,1024,512]{2,1,0:T(8,128)(2,1)} %out_w.1, f32[2,4,257]{2,1,0:T(4,128)} %rel_bias.1), custom_call_target="tpu_custom_call" | custom-call | tf_op jit(solution)/shard_map/pallas_call | solution.py:409
  51.4 1.7 %copy.9 = bf16[256,512]{1,0:T(8,128)(2,1)} copy(bf16[256,512]{1,0:T(8,128)(2,1)} %shard_map.73) | data formatting | bytes 524288
where the time goes:
time: 53.5 us; the launch traced here: 53.1 us
  Pallas kernels  51.4 us (96%)
  local copies, waits for them, and re-layouts  1.67 us (3%)
    pallas_call x1, Pallas kernels, per_device(): pl.pallas_call(functools.partial(kernel, n_tp, n_sp, head_dim), out_shape...  51.4 us
    unnamed x1, local copies, waits for them, and re-layouts  1.67 us

commit v1 on v0

v1 whole, which is shorter than its diff:
```python
import functools

import jax
import jax.numpy as jnp
from jax import lax
from jax.experimental import pallas as pl
from jax.experimental.pallas import tpu as pltpu
from jax.sharding import PartitionSpec as P

SEG = 64
PREV = 8
CLIP = 128
LANES = 128
CHUNKS = 4
DIRECT = 1
PAIR = 2 * SEG
REACH = PREV * SEG
BAND = REACH + PAIR

epsilon = 1e-06
masked_score = -1e30
MESH = pl.DeviceIdType.MESH


class Gather:
    def __init__(self, n_tp, slot, send_sems, recv_sems):
        self.n_x = n_tp // 2
        self.me = lax.axis_index("tp")
        self.core = lax.rem(self.me, 2)
        self.x = self.me // 2
        self.sibling = self.me + 1 - 2 * self.core
        self.slot, self.send_sems, self.recv_sems = slot, send_sems, recv_sems

    def across(self, step, core):
        return lax.rem(self.x + step, self.n_x) * 2 + core

    def copy(self, source, origin, part, index, target):
        return pltpu.make_async_remote_copy(
            src_ref=source,
            dst_ref=self.slot(origin, part),
            send_sem=self.send_sems.at[part, index],
            recv_sem=self.recv_sems.at[part, origin],
            device_id={"tp": target},
            device_id_type=MESH,
        )

    def own(self, part, source=None):
        source = self.slot(self.me, part) if source is None else source
        targets = [self.across(s, self.core) for s in range(1, self.n_x)] + [self.sibling]
        return [self.copy(source, self.me, part, i, t) for i, t in enumerate(targets)]

    def send(self, part, source=None):
        for copy in self.own(part, source):
            copy.start()

    def relays(self, part):
        out = []
        for s in range(1, self.n_x):
            origin = self.across(s, self.core)
            out.append(
                self.copy(self.slot(origin, part), origin, part, self.n_x - 1 + s, self.sibling)
            )
        return out

    def relay(self, part):
        for copy in self.relays(part):
            copy.wait_recv()
            copy.start()

    def others(self):
        return [self.sibling] + [self.across(s, 1 - self.core) for s in range(1, self.n_x)]

    def wait_slot(self, part, origin):
        self.copy(self.slot(origin, part), origin, part, 0, self.sibling).wait_recv()

    def wait_rest(self, part):
        for origin in self.others():
            self.wait_slot(part, origin)

    def finish(self, part, source=None):
        for copy in self.own(part, source) + self.relays(part):
            copy.wait_send()


def kernel(
    n_tp, n_sp, head_dim,
    stream, gain, query_w, key_w, value_w, out_w, rel_bias,
    out,
    xg, gg, table, wkv, wq, wo, normed, bias, edge, qx, kvx, att, top_s, sum_s, mix_s,
    xs, xr, ats, atr, kvs, kvr, gs, gr, wsem, own_sem,
):
    layers, _, rows, width = xg.shape
    head_cols = qx.shape[1]
    groups = head_cols // LANES
    per_group = LANES // head_dim
    total_width = n_tp * width
    shift = REACH // rows
    sp = lax.axis_index("sp")
    tp = lax.axis_index("tp")
    core = lax.rem(tp, 2)
    relayed = shift == 2 and n_sp % 2 == 0
    blocks = rows // PAIR
    piece = rows // CHUNKS
    per_block = CHUNKS // blocks
    heads = per_group * groups
    tall = per_group * PAIR

    key_cols, value_cols = slice(0, head_cols), slice(head_cols, 2 * head_cols)
    weights = []
    for l in range(layers):
        pairs = (
            (key_w, wkv.at[l, :, key_cols]),
            (value_w, wkv.at[l, :, value_cols]),
            (query_w, wq.at[l]),
            (out_w, wo.at[l]),
        )
        weights.append(
            [pltpu.make_async_copy(s.at[l], d, wsem.at[l, i]) for i, (s, d) in enumerate(pairs)]
        )
    own_stream = pltpu.make_async_copy(stream, xg.at[0, tp], own_sem.at[0])
    own_gain = pltpu.make_async_copy(gain, gg.at[tp], own_sem.at[1])
    own_stream.start()
    own_gain.start()
    own_table = pltpu.make_async_copy(rel_bias, table, own_sem.at[2])
    own_table.start()

    barrier = pltpu.get_barrier_semaphore()
    for d in range(1, n_tp):
        pl.semaphore_signal(
            barrier, inc=1, device_id={"tp": lax.rem(tp + d, n_tp)}, device_id_type=MESH
        )
    count = n_tp - 1
    for d in range(1, shift + 1):

        @pl.when(sp + d < n_sp)
        def _():
            pl.semaphore_signal(barrier, inc=1, device_id={"sp": sp + d}, device_id_type=MESH)

        @pl.when(sp >= d)
        def _():
            pl.semaphore_signal(barrier, inc=1, device_id={"sp": sp - d}, device_id_type=MESH)

        count = count + jnp.where(sp + d < n_sp, 1, 0) + jnp.where(sp >= d, 1, 0)
    for copy in weights[0]:
        copy.start()
    with jax.named_scope("barrier"):
        pl.semaphore_wait(barrier, count)

    xgather = [
        Gather(
            n_tp,
            lambda j, c, l=l: xg.at[l, j, pl.ds(c * piece, piece)],
            xs.at[l],
            xr.at[l],
        )
        for l in range(layers)
    ]
    agather = [
        Gather(n_tp, lambda j, p, l=l: att.at[l, j, p], ats.at[l], atr.at[l])
        for l in range(layers)
    ]

    own_stream.wait()
    for c in range(CHUNKS):
        xgather[0].send(c)
    gain_copies = [
        pltpu.make_async_remote_copy(
            src_ref=gain,
            dst_ref=gg.at[tp],
            send_sem=gs.at[d - 1],
            recv_sem=gr.at[d - 1],
            device_id={"tp": lax.rem(tp + d, n_tp)},
            device_id_type=MESH,
        )
        for d in range(1, n_tp)
    ]
    for copy in gain_copies:
        copy.start()
    for l in range(1, layers):
        for copy in weights[l]:
            copy.start()

    for l in range(layers):
        for d in range(1, shift + 1):

            @pl.when(sp < d)
            def _():
                kvx[l, pl.ds((shift - d) * rows, rows), :] = jnp.zeros(
                    (rows, 2 * head_cols), jnp.bfloat16
                )

    near = 2 * CLIP

    def make_bias():
        own_table.wait()
        flip = (
            lax.broadcasted_iota(jnp.int32, (near, near), 0)
            + lax.broadcasted_iota(jnp.int32, (near, near), 1)
            == near - 1
        ).astype(jnp.float32)
        q_row = lax.broadcasted_iota(jnp.int32, (PAIR, PAIR), 0)
        k_col = lax.broadcasted_iota(jnp.int32, (PAIR, PAIR), 1)
        later = (q_row < SEG) & (k_col >= SEG)
        before = (q_row >= SEG) & (k_col < SEG)
        far_hidden = jnp.where(sp >= shift, 0.0, masked_score)
        tile = jnp.where(before, masked_score, far_hidden)
        for h in range(per_group):
            edge[h * PAIR : (h + 1) * PAIR, :] = tile
        for l in range(layers):
            part = table[l]
            turned = jnp.dot(
                part[:, 1:] - part[:, near:], flip, precision=lax.Precision.HIGHEST,
                preferred_element_type=jnp.float32,
            )
            base = jnp.concatenate([turned, jnp.zeros((heads, PAIR), jnp.float32)], axis=1)
            for h in range(heads):
                spread = jnp.broadcast_to(base[h : h + 1], (PAIR, base.shape[1]))
                shifted = pltpu.roll(spread, 0, 1, stride=1, stride_axis=0)
                first = h % per_group * PAIR
                span = slice(first, first + PAIR)
                bias[l, h // per_group, span, :PAIR] = shifted[:, :PAIR]
                bias[l, h // per_group, span, PAIR:] = jnp.where(
                    later, masked_score, shifted[:, PAIR : 2 * PAIR]
                )

    even = lax.rem(sp, 2) == 0
    odd_behind = (lax.rem(sp, 2) == 1) & (sp >= 2)

    def halo_copy(l, c, from_slot, to_slot, index, target):
        return pltpu.make_async_remote_copy(
            src_ref=kvx.at[l, pl.ds(from_slot * rows + c * piece, piece)],
            dst_ref=kvx.at[l, pl.ds(to_slot * rows + c * piece, piece)],
            send_sem=kvs.at[l, c, index],
            recv_sem=kvr.at[l, c, to_slot],
            device_id={"sp": target},
            device_id_type=MESH,
        )

    def is_relayed(c):
        return relayed and c < CHUNKS - DIRECT

    def direct_copies(l, c):
        out_list = []
        for d in range(shift, 0, -1):
            ok = sp + d < n_sp
            if is_relayed(c) and d == 1:
                ok = even
            out_list.append((ok, halo_copy(l, c, shift, shift - d, d - 1, sp + d)))
        return out_list

    def relay_copy(l, c):
        return halo_copy(l, c, 0, 1, shift, sp - 1)

    def halo_send(l, c):
        for ok, copy in direct_copies(l, c):
            pl.when(ok)(copy.start)

    def halo_wait_slot(l, c, d):
        @pl.when(sp >= d)
        def _():
            slot = shift - d
            halo_copy(l, c, slot, slot, 0, lax.rem(sp + 1, n_sp)).wait_recv()

    def halo_far(l, c):
        halo_wait_slot(l, c, shift)
        if is_relayed(c):
            pl.when(odd_behind)(relay_copy(l, c).start)

    def halo_near(l):
        for c in range(CHUNKS):
            for d in range(shift - 1, 0, -1):
                halo_wait_slot(l, c, d)

    def wait_gain():
        own_gain.wait()
        for d in range(1, n_tp):
            pltpu.make_async_remote_copy(
                src_ref=gain,
                dst_ref=gg.at[lax.rem(tp - d + n_tp, n_tp)],
                send_sem=gs.at[d - 1],
                recv_sem=gr.at[d - 1],
                device_id={"tp": lax.rem(tp + d, n_tp)},
                device_id_type=MESH,
            ).wait_recv()

    lane = lax.broadcasted_iota(jnp.int32, (PAIR, LANES), 1) // head_dim
    scale = head_dim ** (-0.5)

    def normalize(l, c):
        span = slice(c * piece, (c + 1) * piece)
        squares = jnp.zeros((piece, 1), jnp.float32)
        for j in range(n_tp):
            part = xg[l, j, span, :].astype(jnp.float32)
            squares = squares + jnp.sum(part * part, axis=-1, keepdims=True)
        inverse = lax.rsqrt(squares / total_width + epsilon)
        for j in range(n_tp):
            part = xg[l, j, span, :].astype(jnp.float32) * inverse
            normed[span, j * width : (j + 1) * width] = (
                part * gg[j, l : l + 1, :]
            ).astype(jnp.bfloat16)

    def block_rows(b):
        return slice(b * PAIR, (b + 1) * PAIR)

    def keys_values(l, c):
        if c == 0:
            weights[l][0].wait()
            weights[l][1].wait()
        span = slice(c * piece, (c + 1) * piece)
        made = jnp.dot(normed[span, :], wkv[l], preferred_element_type=jnp.float32)
        first = REACH + c * piece
        kvx[l, first : first + piece, :] = made.astype(jnp.bfloat16)
        halo_send(l, c)

    def queries(l, b):
        if b == 0:
            weights[l][2].wait()
        qx[block_rows(b), :] = (
            jnp.dot(normed[block_rows(b), :], wq[l], preferred_element_type=jnp.float32) * scale
        ).astype(jnp.bfloat16)

    def scored(l, b, g, spans):
        lanes = slice(g * LANES, (g + 1) * LANES)
        block = qx[block_rows(b), lanes]
        stacked = jnp.concatenate(
            [jnp.where(lane == h, block, jnp.zeros_like(block)) for h in range(per_group)], axis=0
        )
        values_at = slice(head_cols + g * LANES, head_cols + (g + 1) * LANES)
        keys = jnp.concatenate([kvx[l, first:last, lanes] for first, last in spans], axis=0)
        values = jnp.concatenate([kvx[l, first:last, values_at] for first, last in spans], axis=0)
        scores = lax.dot_general(
            stacked, keys, (((1,), (1,)), ((), ())), preferred_element_type=jnp.float32
        )
        tiles = []
        starts = [at for first, last in spans for at in range(first, last, PAIR)]
        for t, at in enumerate(starts):
            tile = scores[:, t * PAIR : (t + 1) * PAIR]
            place = at // PAIR - b
            if place == 0:
                tile = tile + edge[...]
            elif at < REACH:
                behind = shift - at // rows
                tile = tile + jnp.where(sp >= behind, 0.0, masked_score)
            last_tiles = place - (BAND // PAIR - 2)
            if last_tiles >= 0:
                tile = tile + bias[l, g, :, last_tiles * PAIR : (last_tiles + 1) * PAIR]
            tiles.append(tile)
        top = jnp.max(functools.reduce(jnp.maximum, tiles), axis=-1, keepdims=True)
        return tiles, top, values

    def weighed(tiles, top, values):
        grown = [jnp.exp(tile - top) for tile in tiles]
        summed = jnp.sum(functools.reduce(jnp.add, grown), axis=-1, keepdims=True)
        packed = jnp.concatenate([tile.astype(jnp.bfloat16) for tile in grown], axis=1)
        return summed, jnp.dot(packed, values, preferred_element_type=jnp.float32)

    def attend_first(l, b, g):
        unit = b * groups + g
        spans = ((b * PAIR, rows), (REACH, REACH + (b + 1) * PAIR))
        tiles, top, values = scored(l, b, g, spans)
        summed, mix = weighed(tiles, top, values)
        top_s[unit] = top
        sum_s[unit] = summed
        mix_s[unit] = mix

    def attend_rest(l, b, g):
        unit = b * groups + g
        summed, mix = sum_s[unit], mix_s[unit]
        if shift > 1:
            tiles, top, values = scored(l, b, g, ((rows, REACH),))
            before = top_s[unit]
            top = jnp.maximum(top, before)
            more, extra = weighed(tiles, top, values)
            fade = jnp.exp(before - top)
            summed = summed * fade + more
            mix = mix * fade + extra
        mix = mix * (1.0 / summed)
        chosen = mix[:PAIR]
        for h in range(1, per_group):
            chosen = jnp.where(lane == h, mix[h * PAIR : (h + 1) * PAIR], chosen)
        att[l, tp, unit] = chosen.astype(jnp.bfloat16)

    def mixed_part(l, b, j):
        mat = wo[l, pl.ds(pl.multiple_of(j * head_cols, LANES), head_cols), :]
        left = jnp.concatenate([att[l, j, b * groups + g] for g in range(groups)], axis=1)
        return jnp.dot(left, mat, preferred_element_type=jnp.float32)

    def relay_on(gather, parts, which):
        @pl.when(core == which)
        def _():
            for part in parts:
                gather.relay(part)

    with jax.named_scope("bias"):
        make_bias()
    with jax.named_scope("gain"):
        wait_gain()

    for l in range(layers):
        gather = xgather[l]
        with jax.named_scope(f"L{l}xrel0"):
            gather.relay(0)
        for c in range(CHUNKS):
            with jax.named_scope(f"L{l}xwait{c}"):
                if c + 1 < CHUNKS:
                    relay_on(gather, (c + 1,), 1)
                gather.wait_rest(c)
            with jax.named_scope(f"L{l}norm{c}"):
                normalize(l, c)
            with jax.named_scope(f"L{l}kv{c}"):
                keys_values(l, c)
            with jax.named_scope(f"L{l}xrel{c+1}"):
                if c + 1 < CHUNKS:
                    relay_on(gather, (c + 1,), 0)
        for c in range(CHUNKS):
            with jax.named_scope(f"L{l}far{c}"):
                halo_far(l, c)
            if c < blocks:
                with jax.named_scope(f"L{l}q{c}"):
                    queries(l, c)
        for b in range(min(CHUNKS, blocks), blocks):
            queries(l, b)
        with jax.named_scope(f"L{l}attA"):
            for b in range(blocks):
                for g in range(groups):
                    attend_first(l, b, g)
        with jax.named_scope(f"L{l}near"):
            halo_near(l)
        with jax.named_scope(f"L{l}attB"):
            for b in range(blocks):
                for g in range(groups):
                    attend_rest(l, b, g)
                    agather[l].send(b * groups + g)

        gather = agather[l]
        parts = [[b * groups + g for g in range(groups)] for b in range(blocks)]
        with jax.named_scope(f"L{l}arel0"):
            weights[l][3].wait()
            for part in parts[0]:
                gather.relay(part)
        for b in range(blocks):
            with jax.named_scope(f"L{l}own{b}"):
                total = xg[l, tp, block_rows(b), :].astype(jnp.float32) + mixed_part(l, b, tp)
                for s in range(1, gather.n_x):
                    total = total + mixed_part(l, b, gather.across(s, gather.core))
            if b + 1 < blocks:
                with jax.named_scope(f"L{l}arel{b+1}n"):
                    relay_on(gather, parts[b + 1], 1)
            for i, origin in enumerate(gather.others()):
                with jax.named_scope(f"L{l}await{b}{i}"):
                    for part in parts[b]:
                        gather.wait_slot(part, origin)
                total = total + mixed_part(l, b, origin)
            with jax.named_scope(f"L{l}res{b}"):
                result = total.astype(jnp.bfloat16)
                if l + 1 < layers:
                    xg[l + 1, tp, block_rows(b), :] = result
                    for c in range(b * per_block, (b + 1) * per_block):
                        xgather[l + 1].send(c)
                else:
                    out[block_rows(b), :] = result
            if b + 1 < blocks:
                with jax.named_scope(f"L{l}arel{b+1}s"):
                    relay_on(gather, parts[b + 1], 0)

    with jax.named_scope("drain"):
        for copy in gain_copies:
            copy.wait_send()
        for l in range(layers):
            for c in range(CHUNKS):
                xgather[l].finish(c)
                for ok, copy in direct_copies(l, c):
                    pl.when(ok)(copy.wait_send)
                if is_relayed(c):
                    pl.when(odd_behind)(relay_copy(l, c).wait_send)
            for part in range(blocks * groups):
                agather[l].finish(part)


def per_device(n_tp, n_sp, stream, norm_gain, query_weight, key_weight, value_weight, out_weight, rel_bias):
    rows, width = stream.shape
    layers, full, head_cols = query_weight.shape
    heads_here = rel_bias.shape[1]
    head_dim = head_cols // heads_here
    groups = head_cols // LANES
    n_x = n_tp // 2
    shift = REACH // rows
    blocks = rows // PAIR
    tall = (LANES // head_dim) * PAIR
    any_space = pl.BlockSpec(memory_space=pltpu.HBM)
    vmem = pl.BlockSpec(memory_space=pltpu.VMEM)
    bf16, f32 = jnp.bfloat16, jnp.float32
    dma = pltpu.SemaphoreType.DMA
    operands = (stream, norm_gain, query_weight, key_weight, value_weight, out_weight, rel_bias)
    return pl.pallas_call(
        functools.partial(kernel, n_tp, n_sp, head_dim),
        out_shape=jax.ShapeDtypeStruct((rows, width), bf16),
        in_specs=[any_space] * 7,
        out_specs=vmem,
        scratch_shapes=[
            pltpu.VMEM((layers, n_tp, rows, width), bf16),
            pltpu.VMEM((n_tp, layers, width), f32),
            pltpu.VMEM(rel_bias.shape, f32),
            pltpu.VMEM((layers, full, 2 * head_cols), bf16),
            pltpu.VMEM((layers, full, head_cols), bf16),
            pltpu.VMEM((layers, n_tp * head_cols, width), bf16),
            pltpu.VMEM((rows, full), bf16),
            pltpu.VMEM((layers, groups, tall, 2 * PAIR), f32),
            pltpu.VMEM((tall, PAIR), f32),
            pltpu.VMEM((rows, head_cols), bf16),
            pltpu.VMEM((layers, REACH + rows, 2 * head_cols), bf16),
            pltpu.VMEM((layers, n_tp, blocks * groups, PAIR, LANES), bf16),
            pltpu.VMEM((blocks * groups, tall, 1), f32),
            pltpu.VMEM((blocks * groups, tall, 1), f32),
            pltpu.VMEM((blocks * groups, tall, LANES), f32),
            dma((layers, CHUNKS, 2 * n_x - 1)),
            dma((layers, CHUNKS, n_tp)),
            dma((layers, blocks * groups, 2 * n_x - 1)),
            dma((layers, blocks * groups, n_tp)),
            dma((layers, CHUNKS, shift + 1)),
            dma((layers, CHUNKS, shift)),
            dma((n_tp - 1,)),
            dma((n_tp - 1,)),
            dma((layers, 4)),
            dma((3,)),
        ],
        compiler_params=pltpu.CompilerParams(
            collective_id=0, has_side_effects=True, vmem_limit_bytes=40 * 1024 * 1024
        ),
    )(*[pltpu.with_memory_space_constraint(a, pltpu.HBM) for a in operands])


def solution(mesh):
    placed = (
        P("sp", "tp"),
        P(None, "tp"),
        P(None, None, "tp"),
        P(None, None, "tp"),
        P(None, None, "tp"),
        P(None, None, "tp"),
        P(None, "tp", None),
    )
    return jax.shard_map(
        functools.partial(per_device, mesh.shape["tp"], mesh.shape["sp"]),
        mesh=mesh, in_specs=placed, out_specs=P("sp", "tp"), check_vma=False,
    )
```

time: 53.5 us -> 52.1 us (0.974)
  local copies, waits for them, and re-layouts: 1.67 us -> 0.71 us
    unnamed x1, local copies, waits for them, and re-layouts: 1.67 us -> 0.71 us
where the time goes in v1:
time: 52.1 us; the launch traced here: 52 us
  Pallas kernels  51.3 us (98%)
  local copies, waits for them, and re-layouts  0.71 us (1%)
    pallas_call x1, Pallas kernels, per_device(): pl.pallas_call(functools.partial(kernel, n_tp, n_sp, head_dim), out_shape...  51.3 us

profile of v1, /device:TPU:17, one launch (start us, length us, event | category | flops | bytes accessed | tf_op | source)
XLA Modules:
  0.0 52.0 jit_solution(11494030051841746739)
XLA Ops:
  0.0 51.3 %shard_map.73 = bf16[256,512]{1,0:T(8,128)(2,1)S(1)} custom-call(bf16[256,512]{1,0:T(8,128)(2,1)} %stream.1, f32[2,512]{1,0:T(2,128)} %gain.1, bf16[2,2048,256]{2,1,0:T(8,128)(2,1)} %query_w.1, bf16[2,2048,256]{2,1,0:T(8,128)(2,1)} %key_w.1, bf16[2,2048,256]{2,1,0:T(8,128)(2,1)} %value_w.1, bf16[2,1024,512]{2,1,0:T(8,128)(2,1)} %out_w.1, f32[2,4,257]{2,1,0:T(4,128)} %rel_bias.1), custom_call_target="tpu_custom_call" | custom-call | tf_op jit(solution)/shard_map/pallas_call | solution.py:495
  51.3 0.7 %copy.9 = bf16[256,512]{1,0:T(8,128)(2,1)} copy(bf16[256,512]{1,0:T(8,128)(2,1)S(1)} %shard_map.73) | data formatting | bytes 524288

commit v2 on v1

--- a/solution.py
+++ b/solution.py
@@ -12,7 +12,9 @@
 CLIP = 128
 LANES = 128
 CHUNKS = 4
-DIRECT = 1
+PIECES = 8
+EARLY = 1
+LATE = 128
 PAIR = 2 * SEG
 REACH = PREV * SEG
 BAND = REACH + PAIR
@@ -34,9 +36,12 @@
     def across(self, step, core):
         return lax.rem(self.x + step, self.n_x) * 2 + core
 
-    def copy(self, source, origin, part, index, target):
+    def outside(self):
+        return [self.across(s, core) for s in range(1, self.n_x) for core in (1, 0)]
+
+    def copy(self, origin, part, index, target):
         return pltpu.make_async_remote_copy(
-            src_ref=source,
+            src_ref=self.slot(origin, part),
             dst_ref=self.slot(origin, part),
             send_sem=self.send_sems.at[part, index],
             recv_sem=self.recv_sems.at[part, origin],
@@ -44,49 +49,53 @@
             device_id_type=MESH,
         )
 
-    def own(self, part, source=None):
-        source = self.slot(self.me, part) if source is None else source
-        targets = [self.across(s, self.core) for s in range(1, self.n_x)] + [self.sibling]
-        return [self.copy(source, self.me, part, i, t) for i, t in enumerate(targets)]
-
-    def send(self, part, source=None):
-        for copy in self.own(part, source):
+    def own(self, part):
+        targets = [self.sibling] + [self.across(s, 1) for s in range(1, self.n_x)]
+        return [self.copy(self.me, part, i, t) for i, t in enumerate(targets)]
+
+    def send(self, part):
+        for copy in self.own(part):
             copy.start()
 
     def relays(self, part):
-        out = []
-        for s in range(1, self.n_x):
-            origin = self.across(s, self.core)
-            out.append(
-                self.copy(self.slot(origin, part), origin, part, self.n_x - 1 + s, self.sibling)
-            )
-        return out
+        return [
+            self.copy(origin, part, self.n_x + i, self.sibling)
+            for i, origin in enumerate(self.outside())
+        ]
 
     def relay(self, part):
-        for copy in self.relays(part):
-            copy.wait_recv()
-            copy.start()
-
-    def others(self):
-        return [self.sibling] + [self.across(s, 1 - self.core) for s in range(1, self.n_x)]
+        @pl.when(self.core == 1)
+        def _():
+            for copy in self.relays(part):
+                copy.wait_recv()
+                copy.start()
 
     def wait_slot(self, part, origin):
-        self.copy(self.slot(origin, part), origin, part, 0, self.sibling).wait_recv()
+        self.copy(origin, part, 0, self.sibling).wait_recv()
 
     def wait_rest(self, part):
-        for origin in self.others():
-            self.wait_slot(part, origin)
-
-    def finish(self, part, source=None):
-        for copy in self.own(part, source) + self.relays(part):
+        self.wait_slot(part, self.sibling)
+
+        @pl.when(self.core == 0)
+        def _():
+            for origin in self.outside():
+                self.wait_slot(part, origin)
+
+    def finish(self, part):
+        for copy in self.own(part):
             copy.wait_send()
+
+        @pl.when(self.core == 1)
+        def _():
+            for copy in self.relays(part):
+                copy.wait_send()
 
 
 def kernel(
     n_tp, n_sp, head_dim,
     stream, gain, query_w, key_w, value_w, out_w, rel_bias,
     out,
-    xg, gg, table, wkv, wq, wo, normed, bias, edge, qx, kvx, att, top_s, sum_s, mix_s,
+    xg, gg, table, wkv, wq, wo, normed, bias, edge, qx, kvx, att, top_s, mix_s,
     xs, xr, ats, atr, kvs, kvr, gs, gr, wsem, own_sem,
 ):
     layers, _, rows, width = xg.shape
@@ -97,11 +106,12 @@
     shift = REACH // rows
     sp = lax.axis_index("sp")
     tp = lax.axis_index("tp")
-    core = lax.rem(tp, 2)
     relayed = shift == 2 and n_sp % 2 == 0
     blocks = rows // PAIR
     piece = rows // CHUNKS
     per_block = CHUNKS // blocks
+    strip = rows // PIECES
+    per_chunk = PIECES // CHUNKS
     heads = per_group * groups
     tall = per_group * PAIR
 
@@ -130,17 +140,22 @@
             barrier, inc=1, device_id={"tp": lax.rem(tp + d, n_tp)}, device_id_type=MESH
         )
     count = n_tp - 1
+    even = lax.rem(sp, 2) == 0
+    odd_behind = (lax.rem(sp, 2) == 1) & (sp >= 2)
     for d in range(1, shift + 1):
-
-        @pl.when(sp + d < n_sp)
+        pair = even if relayed and d == 1 else sp >= 0
+        ahead = (sp + d < n_sp) & pair
+        behind = (sp >= d) & (~even if relayed and d == 1 else sp >= 0)
+
+        @pl.when(ahead)
         def _():
             pl.semaphore_signal(barrier, inc=1, device_id={"sp": sp + d}, device_id_type=MESH)
 
-        @pl.when(sp >= d)
+        @pl.when(behind)
         def _():
             pl.semaphore_signal(barrier, inc=1, device_id={"sp": sp - d}, device_id_type=MESH)
 
-        count = count + jnp.where(sp + d < n_sp, 1, 0) + jnp.where(sp >= d, 1, 0)
+        count = count + jnp.where(ahead, 1, 0) + jnp.where(behind, 1, 0)
     for copy in weights[0]:
         copy.start()
     with jax.named_scope("barrier"):
@@ -160,12 +175,9 @@
         for l in range(layers)
     ]
 
-    own_stream.wait()
-    for c in range(CHUNKS):
-        xgather[0].send(c)
     gain_copies = [
         pltpu.make_async_remote_copy(
-            src_ref=gain,
+            src_ref=gg.at[tp],
             dst_ref=gg.at[tp],
             send_sem=gs.at[d - 1],
             recv_sem=gr.at[d - 1],
@@ -174,8 +186,12 @@
         )
         for d in range(1, n_tp)
     ]
+    own_gain.wait()
     for copy in gain_copies:
         copy.start()
+    own_stream.wait()
+    for c in range(CHUNKS):
+        xgather[0].send(c)
     for l in range(1, layers):
         for copy in weights[l]:
             copy.start()
@@ -223,28 +239,22 @@
                     later, masked_score, shifted[:, PAIR : 2 * PAIR]
                 )
 
-    even = lax.rem(sp, 2) == 0
-    odd_behind = (lax.rem(sp, 2) == 1) & (sp >= 2)
-
     def halo_copy(l, c, from_slot, to_slot, index, target):
         return pltpu.make_async_remote_copy(
-            src_ref=kvx.at[l, pl.ds(from_slot * rows + c * piece, piece)],
-            dst_ref=kvx.at[l, pl.ds(to_slot * rows + c * piece, piece)],
+            src_ref=kvx.at[l, pl.ds(from_slot * rows + c * strip, strip)],
+            dst_ref=kvx.at[l, pl.ds(to_slot * rows + c * strip, strip)],
             send_sem=kvs.at[l, c, index],
             recv_sem=kvr.at[l, c, to_slot],
             device_id={"sp": target},
             device_id_type=MESH,
         )
 
-    def is_relayed(c):
-        return relayed and c < CHUNKS - DIRECT
-
     def direct_copies(l, c):
         out_list = []
         for d in range(shift, 0, -1):
             ok = sp + d < n_sp
-            if is_relayed(c) and d == 1:
-                ok = even
+            if relayed and d == 1:
+                ok = even & ok
             out_list.append((ok, halo_copy(l, c, shift, shift - d, d - 1, sp + d)))
         return out_list
 
@@ -261,21 +271,31 @@
             slot = shift - d
             halo_copy(l, c, slot, slot, 0, lax.rem(sp + 1, n_sp)).wait_recv()
 
+    def halo_relay(l, c):
+        @pl.when(odd_behind)
+        def _():
+            halo_copy(l, c, 0, 0, 0, lax.rem(sp + 1, n_sp)).wait_recv()
+            relay_copy(l, c).start()
+
     def halo_far(l, c):
-        halo_wait_slot(l, c, shift)
-        if is_relayed(c):
-            pl.when(odd_behind)(relay_copy(l, c).start)
-
-    def halo_near(l):
-        for c in range(CHUNKS):
+        if relayed:
+
+            @pl.when(even & (sp >= 2))
+            def _():
+                halo_copy(l, c, 0, 0, 0, lax.rem(sp + 1, n_sp)).wait_recv()
+
+        else:
+            halo_wait_slot(l, c, shift)
+
+    def halo_near(l, pieces):
+        for c in pieces:
             for d in range(shift - 1, 0, -1):
                 halo_wait_slot(l, c, d)
 
     def wait_gain():
-        own_gain.wait()
         for d in range(1, n_tp):
             pltpu.make_async_remote_copy(
-                src_ref=gain,
+                src_ref=gg.at[tp],
                 dst_ref=gg.at[lax.rem(tp - d + n_tp, n_tp)],
                 send_sem=gs.at[d - 1],
                 recv_sem=gr.at[d - 1],
@@ -310,7 +330,8 @@
         made = jnp.dot(normed[span, :], wkv[l], preferred_element_type=jnp.float32)
         first = REACH + c * piece
         kvx[l, first : first + piece, :] = made.astype(jnp.bfloat16)
-        halo_send(l, c)
+        for p in range(c * per_chunk, (c + 1) * per_chunk):
+            halo_send(l, p)
 
     def queries(l, b):
         if b == 0:
@@ -346,35 +367,28 @@
                 tile = tile + bias[l, g, :, last_tiles * PAIR : (last_tiles + 1) * PAIR]
             tiles.append(tile)
         top = jnp.max(functools.reduce(jnp.maximum, tiles), axis=-1, keepdims=True)
-        return tiles, top, values
+        return tiles, jnp.broadcast_to(top, (tall, LANES)), values
 
     def weighed(tiles, top, values):
-        grown = [jnp.exp(tile - top) for tile in tiles]
-        summed = jnp.sum(functools.reduce(jnp.add, grown), axis=-1, keepdims=True)
-        packed = jnp.concatenate([tile.astype(jnp.bfloat16) for tile in grown], axis=1)
-        return summed, jnp.dot(packed, values, preferred_element_type=jnp.float32)
+        packed = jnp.concatenate([jnp.exp(tile - top).astype(jnp.bfloat16) for tile in tiles], axis=1)
+        beside = jnp.concatenate([values, jnp.ones_like(values)], axis=1)
+        return jnp.dot(packed, beside, preferred_element_type=jnp.float32)
 
     def attend_first(l, b, g):
         unit = b * groups + g
-        spans = ((b * PAIR, rows), (REACH, REACH + (b + 1) * PAIR))
-        tiles, top, values = scored(l, b, g, spans)
-        summed, mix = weighed(tiles, top, values)
+        spans = ((b * PAIR, rows), (rows, REACH - LATE), (REACH, REACH + (b + 1) * PAIR))
+        tiles, top, values = scored(l, b, g, [s for s in spans if s[1] > s[0]])
         top_s[unit] = top
-        sum_s[unit] = summed
-        mix_s[unit] = mix
+        mix_s[unit] = weighed(tiles, top, values)
 
     def attend_rest(l, b, g):
         unit = b * groups + g
-        summed, mix = sum_s[unit], mix_s[unit]
-        if shift > 1:
-            tiles, top, values = scored(l, b, g, ((rows, REACH),))
-            before = top_s[unit]
-            top = jnp.maximum(top, before)
-            more, extra = weighed(tiles, top, values)
-            fade = jnp.exp(before - top)
-            summed = summed * fade + more
-            mix = mix * fade + extra
-        mix = mix * (1.0 / summed)
+        tiles, top, values = scored(l, b, g, ((REACH - LATE, REACH),))
+        before = top_s[unit]
+        top = jnp.maximum(top, before)
+        fade = jnp.exp(before - top)
+        mix = mix_s[unit] * jnp.concatenate([fade, fade], axis=1) + weighed(tiles, top, values)
+        mix = mix[:, :LANES] / mix[:, LANES:]
         chosen = mix[:PAIR]
         for h in range(1, per_group):
             chosen = jnp.where(lane == h, mix[h * PAIR : (h + 1) * PAIR], chosen)
@@ -385,12 +399,6 @@
         left = jnp.concatenate([att[l, j, b * groups + g] for g in range(groups)], axis=1)
         return jnp.dot(left, mat, preferred_element_type=jnp.float32)
 
-    def relay_on(gather, parts, which):
-        @pl.when(core == which)
-        def _():
-            for part in parts:
-                gather.relay(part)
-
     with jax.named_scope("bias"):
         make_bias()
     with jax.named_scope("gain"):
@@ -398,60 +406,64 @@
 
     for l in range(layers):
         gather = xgather[l]
-        with jax.named_scope(f"L{l}xrel0"):
-            gather.relay(0)
         for c in range(CHUNKS):
+            with jax.named_scope(f"L{l}xrel{c}"):
+                gather.relay(c)
             with jax.named_scope(f"L{l}xwait{c}"):
-                if c + 1 < CHUNKS:
-                    relay_on(gather, (c + 1,), 1)
                 gather.wait_rest(c)
             with jax.named_scope(f"L{l}norm{c}"):
                 normalize(l, c)
             with jax.named_scope(f"L{l}kv{c}"):
                 keys_values(l, c)
-            with jax.named_scope(f"L{l}xrel{c+1}"):
-                if c + 1 < CHUNKS:
-                    relay_on(gather, (c + 1,), 0)
-        for c in range(CHUNKS):
-            with jax.named_scope(f"L{l}far{c}"):
-                halo_far(l, c)
-            if c < blocks:
-                with jax.named_scope(f"L{l}q{c}"):
-                    queries(l, c)
-        for b in range(min(CHUNKS, blocks), blocks):
-            queries(l, b)
+            if relayed and c + 2 == CHUNKS:
+                with jax.named_scope(f"L{l}hrel0"):
+                    for p in range(EARLY):
+                        halo_relay(l, p)
+        for b in range(blocks):
+            for p in range(EARLY + b, EARLY + b + 1):
+                if relayed:
+                    with jax.named_scope(f"L{l}hrel{p}"):
+                        halo_relay(l, p)
+            with jax.named_scope(f"L{l}q{b}"):
+                queries(l, b)
+        if relayed:
+            for p in range(EARLY + blocks, PIECES):
+                with jax.named_scope(f"L{l}hrel{p}"):
+                    halo_relay(l, p)
+        split = (REACH - LATE - (shift - 1) * rows) // strip
+        with jax.named_scope(f"L{l}far"):
+            for p in range(PIECES):
+                halo_far(l, p)
+        with jax.named_scope(f"L{l}near0"):
+            halo_near(l, range(split))
         with jax.named_scope(f"L{l}attA"):
             for b in range(blocks):
                 for g in range(groups):
                     attend_first(l, b, g)
         with jax.named_scope(f"L{l}near"):
-            halo_near(l)
+            halo_near(l, range(split, PIECES))
         with jax.named_scope(f"L{l}attB"):
             for b in range(blocks):
                 for g in range(groups):
                     attend_rest(l, b, g)
+                for g in range(groups):
                     agather[l].send(b * groups + g)
 
         gather = agather[l]
         parts = [[b * groups + g for g in range(groups)] for b in range(blocks)]
-        with jax.named_scope(f"L{l}arel0"):
-            weights[l][3].wait()
-            for part in parts[0]:
-                gather.relay(part)
+        weights[l][3].wait()
         for b in range(blocks):
             with jax.named_scope(f"L{l}own{b}"):
                 total = xg[l, tp, block_rows(b), :].astype(jnp.float32) + mixed_part(l, b, tp)
-                for s in range(1, gather.n_x):
-                    total = total + mixed_part(l, b, gather.across(s, gather.core))
-            if b + 1 < blocks:
-                with jax.named_scope(f"L{l}arel{b+1}n"):
-                    relay_on(gather, parts[b + 1], 1)
-            for i, origin in enumerate(gather.others()):
-                with jax.named_scope(f"L{l}await{b}{i}"):
-                    for part in parts[b]:
-                        gather.wait_slot(part, origin)
-                total = total + mixed_part(l, b, origin)
+            with jax.named_scope(f"L{l}arel{b}"):
+                for part in parts[b]:
+                    gather.relay(part)
+            with jax.named_scope(f"L{l}await{b}"):
+                for part in parts[b]:
+                    gather.wait_rest(part)
             with jax.named_scope(f"L{l}res{b}"):
+                for origin in [gather.sibling] + gather.outside():
+                    total = total + mixed_part(l, b, origin)
                 result = total.astype(jnp.bfloat16)
                 if l + 1 < layers:
                     xg[l + 1, tp, block_rows(b), :] = result
@@ -459,9 +471,6 @@
                         xgather[l + 1].send(c)
                 else:
                     out[block_rows(b), :] = result
-            if b + 1 < blocks:
-                with jax.named_scope(f"L{l}arel{b+1}s"):
-                    relay_on(gather, parts[b + 1], 0)
 
     with jax.named_scope("drain"):
         for copy in gain_copies:
@@ -469,10 +478,11 @@
         for l in range(layers):
             for c in range(CHUNKS):
                 xgather[l].finish(c)
-                for ok, copy in direct_copies(l, c):
+            for p in range(PIECES):
+                for ok, copy in direct_copies(l, p):
                     pl.when(ok)(copy.wait_send)
-                if is_relayed(c):
-                    pl.when(odd_behind)(relay_copy(l, c).wait_send)
+                if relayed:
+                    pl.when(odd_behind)(relay_copy(l, p).wait_send)
             for part in range(blocks * groups):
                 agather[l].finish(part)
 
@@ -510,15 +520,14 @@
             pltpu.VMEM((rows, head_cols), bf16),
             pltpu.VMEM((layers, REACH + rows, 2 * head_cols), bf16),
             pltpu.VMEM((layers, n_tp, blocks * groups, PAIR, LANES), bf16),
-            pltpu.VMEM((blocks * groups, tall, 1), f32),
-            pltpu.VMEM((blocks * groups, tall, 1), f32),
             pltpu.VMEM((blocks * groups, tall, LANES), f32),
-            dma((layers, CHUNKS, 2 * n_x - 1)),
+            pltpu.VMEM((blocks * groups, tall, 2 * LANES), f32),
+            dma((layers, CHUNKS, 3 * n_x - 2)),
             dma((layers, CHUNKS, n_tp)),
-            dma((layers, blocks * groups, 2 * n_x - 1)),
+            dma((layers, blocks * groups, 3 * n_x - 2)),
             dma((layers, blocks * groups, n_tp)),
-            dma((layers, CHUNKS, shift + 1)),
-            dma((layers, CHUNKS, shift)),
+            dma((layers, PIECES, shift + 1)),
+            dma((layers, PIECES, shift)),
             dma((n_tp - 1,)),
             dma((n_tp - 1,)),
             dma((layers, 4)),

time: 52.1 us -> 43.9 us (0.84)
  Pallas kernels: 51.3 us -> 43 us
    pallas_call x1, Pallas kernels: 51.3 us -> 43 us  [per_device(): pl.pallas_call(functools.partial(kernel, n_tp, n_sp, head_dim), out_shape...]
where the time goes in v2:
time: 43.9 us; the launch traced here: 43.7 us
  Pallas kernels  43 us (98%)
  local copies, waits for them, and re-layouts  0.71 us (2%)
    pallas_call x1, Pallas kernels, per_device(): pl.pallas_call(functools.partial(kernel, n_tp, n_sp, head_dim), out_shape...  43 us

profile of v2, /device:TPU:17, one launch (start us, length us, event | category | flops | bytes accessed | tf_op | source)
XLA Modules:
  0.0 43.7 jit_solution(12263332173511783874)
XLA Ops:
  0.0 43.0 %shard_map.73 = bf16[256,512]{1,0:T(8,128)(2,1)S(1)} custom-call(bf16[256,512]{1,0:T(8,128)(2,1)} %stream.1, f32[2,512]{1,0:T(2,128)} %gain.1, bf16[2,2048,256]{2,1,0:T(8,128)(2,1)} %query_w.1, bf16[2,2048,256]{2,1,0:T(8,128)(2,1)} %key_w.1, bf16[2,2048,256]{2,1,0:T(8,128)(2,1)} %value_w.1, bf16[2,1024,512]{2,1,0:T(8,128)(2,1)} %out_w.1, f32[2,4,257]{2,1,0:T(4,128)} %rel_bias.1), custom_call_target="tpu_custom_call" | custom-call | tf_op jit(solution)/shard_map/pallas_call | solution.py:505
  43.0 0.7 %copy.9 = bf16[256,512]{1,0:T(8,128)(2,1)} copy(bf16[256,512]{1,0:T(8,128)(2,1)S(1)} %shard_map.73) | data formatting | bytes 524288

commit v3 on v2

--- a/solution.py
+++ b/solution.py
@@ -11,10 +11,10 @@
 PREV = 8
 CLIP = 128
 LANES = 128
-CHUNKS = 4
-PIECES = 8
+STRIP = 32
+CHUNK = 64
+FIRST = 64
 EARLY = 1
-LATE = 128
 PAIR = 2 * SEG
 REACH = PREV * SEG
 BAND = REACH + PAIR
@@ -25,13 +25,14 @@
 
 
 class Gather:
-    def __init__(self, n_tp, slot, send_sems, recv_sems):
-        self.n_x = n_tp // 2
+    def __init__(self, n_tp, buf, layer, spans, send_sems, recv_sems):
+        self.n_tp, self.n_x = n_tp, n_tp // 2
         self.me = lax.axis_index("tp")
         self.core = lax.rem(self.me, 2)
         self.x = self.me // 2
         self.sibling = self.me + 1 - 2 * self.core
-        self.slot, self.send_sems, self.recv_sems = slot, send_sems, recv_sems
+        self.buf, self.layer, self.spans = buf, layer, spans
+        self.send_sems, self.recv_sems = send_sems, recv_sems
 
     def across(self, step, core):
         return lax.rem(self.x + step, self.n_x) * 2 + core
@@ -39,19 +40,21 @@
     def outside(self):
         return [self.across(s, core) for s in range(1, self.n_x) for core in (1, 0)]
 
-    def copy(self, origin, part, index, target):
+    def copy(self, first, count, part, index, target):
+        start, stop = (0, self.buf.shape[2]) if part is None else self.spans[part]
+        block = self.buf.at[self.layer, pl.ds(first, count), pl.ds(start, stop - start)]
         return pltpu.make_async_remote_copy(
-            src_ref=self.slot(origin, part),
-            dst_ref=self.slot(origin, part),
-            send_sem=self.send_sems.at[part, index],
-            recv_sem=self.recv_sems.at[part, origin],
+            src_ref=block,
+            dst_ref=block,
+            send_sem=self.send_sems.at[index],
+            recv_sem=self.recv_sems.at[part or 0],
             device_id={"tp": target},
             device_id_type=MESH,
         )
 
     def own(self, part):
         targets = [self.sibling] + [self.across(s, 1) for s in range(1, self.n_x)]
-        return [self.copy(self.me, part, i, t) for i, t in enumerate(targets)]
+        return [self.copy(self.me, 1, part, i, t) for i, t in enumerate(targets)]
 
     def send(self, part):
         for copy in self.own(part):
@@ -59,35 +62,25 @@
 
     def relays(self, part):
         return [
-            self.copy(origin, part, self.n_x + i, self.sibling)
-            for i, origin in enumerate(self.outside())
+            self.copy(self.across(s, 0), 2, part, self.n_x + s - 1, self.sibling)
+            for s in range(1, self.n_x)
         ]
 
-    def relay(self, part):
+    def take(self, part):
+        self.copy(0, self.n_tp - 1, part, 0, self.sibling).wait_recv()
+
         @pl.when(self.core == 1)
         def _():
             for copy in self.relays(part):
-                copy.wait_recv()
                 copy.start()
 
-    def wait_slot(self, part, origin):
-        self.copy(origin, part, 0, self.sibling).wait_recv()
-
-    def wait_rest(self, part):
-        self.wait_slot(part, self.sibling)
-
-        @pl.when(self.core == 0)
-        def _():
-            for origin in self.outside():
-                self.wait_slot(part, origin)
-
-    def finish(self, part):
-        for copy in self.own(part):
+    def finish(self):
+        for copy in self.own(None):
             copy.wait_send()
 
         @pl.when(self.core == 1)
         def _():
-            for copy in self.relays(part):
+            for copy in self.relays(None):
                 copy.wait_send()
 
 
@@ -96,7 +89,7 @@
     stream, gain, query_w, key_w, value_w, out_w, rel_bias,
     out,
     xg, gg, table, wkv, wq, wo, normed, bias, edge, qx, kvx, att, top_s, mix_s,
-    xs, xr, ats, atr, kvs, kvr, gs, gr, wsem, own_sem,
+    xs, xr, ats, atr, kvs, far_sem, near_sem, gain_sem, wsem, own_sem,
 ):
     layers, _, rows, width = xg.shape
     head_cols = qx.shape[1]
@@ -108,10 +101,10 @@
     tp = lax.axis_index("tp")
     relayed = shift == 2 and n_sp % 2 == 0
     blocks = rows // PAIR
-    piece = rows // CHUNKS
-    per_block = CHUNKS // blocks
-    strip = rows // PIECES
-    per_chunk = PIECES // CHUNKS
+    half = rows // 2
+    cuts = [0] + list(range(FIRST, rows, CHUNK)) + [rows]
+    chunks = list(zip(cuts[:-1], cuts[1:]))
+    pieces = rows // STRIP
     heads = per_group * groups
     tall = per_group * PAIR
 
@@ -125,7 +118,7 @@
             (out_w, wo.at[l]),
         )
         weights.append(
-            [pltpu.make_async_copy(s.at[l], d, wsem.at[l, i]) for i, (s, d) in enumerate(pairs)]
+            [pltpu.make_async_copy(s.at[l], d, wsem.at[l, max(i - 1, 0)]) for i, (s, d) in enumerate(pairs)]
         )
     own_stream = pltpu.make_async_copy(stream, xg.at[0, tp], own_sem.at[0])
     own_gain = pltpu.make_async_copy(gain, gg.at[tp], own_sem.at[1])
@@ -161,36 +154,36 @@
     with jax.named_scope("barrier"):
         pl.semaphore_wait(barrier, count)
 
-    xgather = [
-        Gather(
-            n_tp,
-            lambda j, c, l=l: xg.at[l, j, pl.ds(c * piece, piece)],
-            xs.at[l],
-            xr.at[l],
-        )
-        for l in range(layers)
-    ]
-    agather = [
-        Gather(n_tp, lambda j, p, l=l: att.at[l, j, p], ats.at[l], atr.at[l])
-        for l in range(layers)
-    ]
+    xgather = [Gather(n_tp, xg, l, chunks, xs, xr.at[l]) for l in range(layers)]
+    units = blocks * groups
+    shares = [(b * groups, (b + 1) * groups) for b in range(blocks)]
+    agather = [Gather(n_tp, att, l, shares, ats, atr.at[l]) for l in range(layers)]
 
     gain_copies = [
         pltpu.make_async_remote_copy(
             src_ref=gg.at[tp],
             dst_ref=gg.at[tp],
-            send_sem=gs.at[d - 1],
-            recv_sem=gr.at[d - 1],
+            send_sem=gain_sem.at[0],
+            recv_sem=gain_sem.at[1],
             device_id={"tp": lax.rem(tp + d, n_tp)},
             device_id_type=MESH,
         )
         for d in range(1, n_tp)
     ]
+    other_gains = gg.at[pl.ds(0, n_tp - 1)]
+    all_gains = pltpu.make_async_remote_copy(
+        src_ref=other_gains,
+        dst_ref=other_gains,
+        send_sem=gain_sem.at[0],
+        recv_sem=gain_sem.at[1],
+        device_id={"tp": lax.rem(tp + 1, n_tp)},
+        device_id_type=MESH,
+    )
     own_gain.wait()
     for copy in gain_copies:
         copy.start()
     own_stream.wait()
-    for c in range(CHUNKS):
+    for c in range(len(chunks)):
         xgather[0].send(c)
     for l in range(1, layers):
         for copy in weights[l]:
@@ -239,76 +232,87 @@
                     later, masked_score, shifted[:, PAIR : 2 * PAIR]
                 )
 
-    def halo_copy(l, c, from_slot, to_slot, index, target):
+    def halo_copy(l, p, from_slot, to_slot, index, target):
+        first, size = (0, rows) if p is None else (p * STRIP, STRIP)
+        p = p or 0
+        if to_slot == 0:
+            arrived = far_sem.at[l, p]
+        else:
+            arrived = near_sem.at[l, to_slot - 1, p * STRIP // half]
         return pltpu.make_async_remote_copy(
-            src_ref=kvx.at[l, pl.ds(from_slot * rows + c * strip, strip)],
-            dst_ref=kvx.at[l, pl.ds(to_slot * rows + c * strip, strip)],
-            send_sem=kvs.at[l, c, index],
-            recv_sem=kvr.at[l, c, to_slot],
+            src_ref=kvx.at[l, pl.ds(from_slot * rows + first, size)],
+            dst_ref=kvx.at[l, pl.ds(to_slot * rows + first, size)],
+            send_sem=kvs.at[index],
+            recv_sem=arrived,
             device_id={"sp": target},
             device_id_type=MESH,
         )
 
-    def direct_copies(l, c):
+    def direct_copies(l, p):
         out_list = []
         for d in range(shift, 0, -1):
             ok = sp + d < n_sp
             if relayed and d == 1:
                 ok = even & ok
-            out_list.append((ok, halo_copy(l, c, shift, shift - d, d - 1, sp + d)))
+            out_list.append((ok, halo_copy(l, p, shift, shift - d, d - 1, sp + d)))
         return out_list
 
-    def relay_copy(l, c):
-        return halo_copy(l, c, 0, 1, shift, sp - 1)
-
-    def halo_send(l, c):
-        for ok, copy in direct_copies(l, c):
+    def relay_copy(l, p):
+        return halo_copy(l, p, 0, 1, shift, sp - 1)
+
+    def halo_send(l, p):
+        for ok, copy in direct_copies(l, p):
             pl.when(ok)(copy.start)
 
-    def halo_wait_slot(l, c, d):
-        @pl.when(sp >= d)
+    def halo_finish(l):
+        for ok, copy in direct_copies(l, None):
+            pl.when(ok)(copy.wait_send)
+        if relayed:
+            pl.when(odd_behind)(relay_copy(l, None).wait_send)
+
+    def far_wait(l, p):
+        halo_copy(l, p, 0, 0, 0, lax.rem(sp + 1, n_sp)).wait_recv()
+
+    def halo_relay(l, p):
+        if relayed:
+
+            @pl.when(odd_behind)
+            def _():
+                far_wait(l, p)
+                relay_copy(l, p).start()
+
+    def halo_far(l, which):
+        here = sp >= shift
+        if relayed:
+            here = here & even
+
+        @pl.when(here)
         def _():
+            for p in range(which * half // STRIP, (which + 1) * half // STRIP):
+                far_wait(l, p)
+
+    def halo_near(l, which):
+        for d in range(shift - 1, 0, -1):
             slot = shift - d
-            halo_copy(l, c, slot, slot, 0, lax.rem(sp + 1, n_sp)).wait_recv()
-
-    def halo_relay(l, c):
-        @pl.when(odd_behind)
-        def _():
-            halo_copy(l, c, 0, 0, 0, lax.rem(sp + 1, n_sp)).wait_recv()
-            relay_copy(l, c).start()
-
-    def halo_far(l, c):
-        if relayed:
-
-            @pl.when(even & (sp >= 2))
+
+            @pl.when(sp >= d)
             def _():
-                halo_copy(l, c, 0, 0, 0, lax.rem(sp + 1, n_sp)).wait_recv()
-
-        else:
-            halo_wait_slot(l, c, shift)
-
-    def halo_near(l, pieces):
-        for c in pieces:
-            for d in range(shift - 1, 0, -1):
-                halo_wait_slot(l, c, d)
-
-    def wait_gain():
-        for d in range(1, n_tp):
-            pltpu.make_async_remote_copy(
-                src_ref=gg.at[tp],
-                dst_ref=gg.at[lax.rem(tp - d + n_tp, n_tp)],
-                send_sem=gs.at[d - 1],
-                recv_sem=gr.at[d - 1],
-                device_id={"tp": lax.rem(tp + d, n_tp)},
-                device_id_type=MESH,
-            ).wait_recv()
+                part = kvx.at[l, pl.ds(slot * rows + which * half, half)]
+                pltpu.make_async_remote_copy(
+                    src_ref=part,
+                    dst_ref=part,
+                    send_sem=kvs.at[0],
+                    recv_sem=near_sem.at[l, slot - 1, which],
+                    device_id={"sp": lax.rem(sp + 1, n_sp)},
+                    device_id_type=MESH,
+                ).wait_recv()
 
     lane = lax.broadcasted_iota(jnp.int32, (PAIR, LANES), 1) // head_dim
     scale = head_dim ** (-0.5)
 
     def normalize(l, c):
-        span = slice(c * piece, (c + 1) * piece)
-        squares = jnp.zeros((piece, 1), jnp.float32)
+        span = slice(*chunks[c])
+        squares = jnp.zeros((span.stop - span.start, 1), jnp.float32)
         for j in range(n_tp):
             part = xg[l, j, span, :].astype(jnp.float32)
             squares = squares + jnp.sum(part * part, axis=-1, keepdims=True)
@@ -323,14 +327,14 @@
         return slice(b * PAIR, (b + 1) * PAIR)
 
     def keys_values(l, c):
+        start, stop = chunks[c]
         if c == 0:
-            weights[l][0].wait()
-            weights[l][1].wait()
-        span = slice(c * piece, (c + 1) * piece)
-        made = jnp.dot(normed[span, :], wkv[l], preferred_element_type=jnp.float32)
-        first = REACH + c * piece
-        kvx[l, first : first + piece, :] = made.astype(jnp.bfloat16)
-        for p in range(c * per_chunk, (c + 1) * per_chunk):
+            pltpu.make_async_copy(wkv.at[l], wkv.at[l], wsem.at[l, 0]).wait()
+            if l > 0:
+                halo_finish(l - 1)
+        made = jnp.dot(normed[start:stop, :], wkv[l], preferred_element_type=jnp.float32)
+        kvx[l, REACH + start : REACH + stop, :] = made.astype(jnp.bfloat16)
+        for p in range(start // STRIP, stop // STRIP):
             halo_send(l, p)
 
     def queries(l, b):
@@ -376,14 +380,16 @@
 
     def attend_first(l, b, g):
         unit = b * groups + g
-        spans = ((b * PAIR, rows), (rows, REACH - LATE), (REACH, REACH + (b + 1) * PAIR))
+        spans = [(max(b * PAIR, at), at + half) for at in range(0, REACH, rows)]
+        spans.append((REACH, REACH + (b + 1) * PAIR))
         tiles, top, values = scored(l, b, g, [s for s in spans if s[1] > s[0]])
         top_s[unit] = top
         mix_s[unit] = weighed(tiles, top, values)
 
     def attend_rest(l, b, g):
         unit = b * groups + g
-        tiles, top, values = scored(l, b, g, ((REACH - LATE, REACH),))
+        spans = [(max(b * PAIR, at + half), at + rows) for at in range(0, REACH, rows)]
+        tiles, top, values = scored(l, b, g, spans)
         before = top_s[unit]
         top = jnp.maximum(top, before)
         fade = jnp.exp(before - top)
@@ -402,89 +408,90 @@
     with jax.named_scope("bias"):
         make_bias()
     with jax.named_scope("gain"):
-        wait_gain()
+        all_gains.wait_recv()
 
     for l in range(layers):
         gather = xgather[l]
-        for c in range(CHUNKS):
-            with jax.named_scope(f"L{l}xrel{c}"):
-                gather.relay(c)
-            with jax.named_scope(f"L{l}xwait{c}"):
-                gather.wait_rest(c)
+        for c in range(len(chunks)):
+            with jax.named_scope(f"L{l}xtake{c}"):
+                gather.take(c)
             with jax.named_scope(f"L{l}norm{c}"):
                 normalize(l, c)
             with jax.named_scope(f"L{l}kv{c}"):
                 keys_values(l, c)
-            if relayed and c + 2 == CHUNKS:
-                with jax.named_scope(f"L{l}hrel0"):
+            if c + 2 == len(chunks):
+                with jax.named_scope(f"L{l}hrelE"):
                     for p in range(EARLY):
                         halo_relay(l, p)
         for b in range(blocks):
-            for p in range(EARLY + b, EARLY + b + 1):
-                if relayed:
-                    with jax.named_scope(f"L{l}hrel{p}"):
-                        halo_relay(l, p)
+            with jax.named_scope(f"L{l}hrel{EARLY+b}"):
+                halo_relay(l, EARLY + b)
             with jax.named_scope(f"L{l}q{b}"):
                 queries(l, b)
-        if relayed:
-            for p in range(EARLY + blocks, PIECES):
-                with jax.named_scope(f"L{l}hrel{p}"):
-                    halo_relay(l, p)
-        split = (REACH - LATE - (shift - 1) * rows) // strip
-        with jax.named_scope(f"L{l}far"):
-            for p in range(PIECES):
-                halo_far(l, p)
+        turn = half // STRIP
+        steps = [range(EARLY + blocks, turn)]
+        if l == 0:
+            spare = (pieces - turn) // blocks
+            steps += [range(turn + b * spare, turn + (b + 1) * spare) for b in range(blocks)]
+            steps.append(range(turn + blocks * spare, pieces))
+        else:
+            steps[0] = range(EARLY + blocks, pieces)
+            steps += [()] * (blocks + 1)
+        with jax.named_scope(f"L{l}hrelM"):
+            for p in steps[0]:
+                halo_relay(l, p)
+        with jax.named_scope(f"L{l}far0"):
+            halo_far(l, 0)
         with jax.named_scope(f"L{l}near0"):
-            halo_near(l, range(split))
-        with jax.named_scope(f"L{l}attA"):
-            for b in range(blocks):
+            halo_near(l, 0)
+        for b in range(blocks):
+            with jax.named_scope(f"L{l}A{b}"):
                 for g in range(groups):
                     attend_first(l, b, g)
-        with jax.named_scope(f"L{l}near"):
-            halo_near(l, range(split, PIECES))
-        with jax.named_scope(f"L{l}attB"):
-            for b in range(blocks):
+            with jax.named_scope(f"L{l}hrelA{b}"):
+                for p in steps[b + 1]:
+                    halo_relay(l, p)
+        with jax.named_scope(f"L{l}hrelZ"):
+            for p in steps[-1]:
+                halo_relay(l, p)
+        with jax.named_scope(f"L{l}far1"):
+            halo_far(l, 1)
+        with jax.named_scope(f"L{l}near1"):
+            halo_near(l, 1)
+        if l > 0:
+            agather[l - 1].finish()
+        for b in range(blocks):
+            with jax.named_scope(f"L{l}B{b}"):
                 for g in range(groups):
                     attend_rest(l, b, g)
-                for g in range(groups):
-                    agather[l].send(b * groups + g)
+            agather[l].send(b)
 
         gather = agather[l]
-        parts = [[b * groups + g for g in range(groups)] for b in range(blocks)]
         weights[l][3].wait()
         for b in range(blocks):
             with jax.named_scope(f"L{l}own{b}"):
                 total = xg[l, tp, block_rows(b), :].astype(jnp.float32) + mixed_part(l, b, tp)
-            with jax.named_scope(f"L{l}arel{b}"):
-                for part in parts[b]:
-                    gather.relay(part)
-            with jax.named_scope(f"L{l}await{b}"):
-                for part in parts[b]:
-                    gather.wait_rest(part)
+            with jax.named_scope(f"L{l}atake{b}"):
+                gather.take(b)
             with jax.named_scope(f"L{l}res{b}"):
                 for origin in [gather.sibling] + gather.outside():
                     total = total + mixed_part(l, b, origin)
                 result = total.astype(jnp.bfloat16)
                 if l + 1 < layers:
+                    if b == 0:
+                        xgather[l].finish()
                     xg[l + 1, tp, block_rows(b), :] = result
-                    for c in range(b * per_block, (b + 1) * per_block):
-                        xgather[l + 1].send(c)
+                    for c, (_, stop) in enumerate(chunks):
+                        if b * PAIR < stop <= (b + 1) * PAIR:
+                            xgather[l + 1].send(c)
                 else:
                     out[block_rows(b), :] = result
 
     with jax.named_scope("drain"):
-        for copy in gain_copies:
-            copy.wait_send()
-        for l in range(layers):
-            for c in range(CHUNKS):
-                xgather[l].finish(c)
-            for p in range(PIECES):
-                for ok, copy in direct_copies(l, p):
-                    pl.when(ok)(copy.wait_send)
-                if relayed:
-                    pl.when(odd_behind)(relay_copy(l, p).wait_send)
-            for part in range(blocks * groups):
-                agather[l].finish(part)
+        all_gains.wait_send()
+        xgather[layers - 1].finish()
+        agather[layers - 1].finish()
+        halo_finish(layers - 1)
 
 
 def per_device(n_tp, n_sp, stream, norm_gain, query_weight, key_weight, value_weight, out_weight, rel_bias):
@@ -497,6 +504,7 @@
     shift = REACH // rows
     blocks = rows // PAIR
     tall = (LANES // head_dim) * PAIR
+    chunk_count = len(range(FIRST, rows, CHUNK)) + 1
     any_space = pl.BlockSpec(memory_space=pltpu.HBM)
     vmem = pl.BlockSpec(memory_space=pltpu.VMEM)
     bf16, f32 = jnp.bfloat16, jnp.float32
@@ -522,15 +530,15 @@
             pltpu.VMEM((layers, n_tp, blocks * groups, PAIR, LANES), bf16),
             pltpu.VMEM((blocks * groups, tall, LANES), f32),
             pltpu.VMEM((blocks * groups, tall, 2 * LANES), f32),
-            dma((layers, CHUNKS, 3 * n_x - 2)),
-            dma((layers, CHUNKS, n_tp)),
-            dma((layers, blocks * groups, 3 * n_x - 2)),
-            dma((layers, blocks * groups, n_tp)),
-            dma((layers, PIECES, shift + 1)),
-            dma((layers, PIECES, shift)),
-            dma((n_tp - 1,)),
-            dma((n_tp - 1,)),
-            dma((layers, 4)),
+            dma((2 * n_x - 1,)),
+            dma((layers, chunk_count)),
+            dma((2 * n_x - 1,)),
+            dma((layers, blocks)),
+            dma((shift + 1,)),
+            dma((layers, rows // STRIP)),
+            dma((layers, max(shift - 1, 1), 2)),
+            dma((2,)),
+            dma((layers, 3)),
             dma((3,)),
         ],
         compiler_params=pltpu.CompilerParams(

time: 43.9 us -> 41.4 us (0.943)
  Pallas kernels: 43 us -> 40.5 us
    pallas_call x1, Pallas kernels: 43 us -> 40.5 us  [per_device(): pl.pallas_call(functools.partial(kernel, n_tp, n_sp, head_dim), out_shape...]
where the time goes in v3:
time: 41.4 us; the launch traced here: 41.2 us
  Pallas kernels  40.5 us (98%)
  local copies, waits for them, and re-layouts  0.71 us (2%)
    pallas_call x1, Pallas kernels, per_device(): pl.pallas_call(functools.partial(kernel, n_tp, n_sp, head_dim), out_shape...  40.5 us

profile of v3, /device:TPU:17, one launch (start us, length us, event | category | flops | bytes accessed | tf_op | source)
XLA Modules:
  0.0 41.2 jit_solution(9636036500842980425)
XLA Ops:
  0.0 40.5 %shard_map.73 = bf16[256,512]{1,0:T(8,128)(2,1)S(1)} custom-call(bf16[256,512]{1,0:T(8,128)(2,1)} %stream.1, f32[2,512]{1,0:T(2,128)} %gain.1, bf16[2,2048,256]{2,1,0:T(8,128)(2,1)} %query_w.1, bf16[2,2048,256]{2,1,0:T(8,128)(2,1)} %key_w.1, bf16[2,2048,256]{2,1,0:T(8,128)(2,1)} %value_w.1, bf16[2,1024,512]{2,1,0:T(8,128)(2,1)} %out_w.1, f32[2,4,257]{2,1,0:T(4,128)} %rel_bias.1), custom_call_target="tpu_custom_call" | custom-call | tf_op jit(solution)/shard_map/pallas_call | solution.py:513
  40.5 0.7 %copy.9 = bf16[256,512]{1,0:T(8,128)(2,1)} copy(bf16[256,512]{1,0:T(8,128)(2,1)S(1)} %shard_map.73) | data formatting | bytes 524288
